TPU v7x, 32 devices: a whole 2x2x4 slice. The times are simulated.
32 devices in a mesh: ra: 8 (over z, y), cb: 4 (over x, core).
Axes of the slice: x: 2, y: 2, z: 4, core: 2. Of those that a mesh axis runs over, the one named last changes fastest.
Arguments:
- activations: bfloat16 [512, 4224], P('cb', 'ra'), may hold values from -160 to 160, as said below
- norm_gain: float32 [2, 4224], replicated, may hold values from 0.1 to 1.9
- gate_weight: float32 [2, 4224, 11520], P(None, None, 'ra'), may hold values from -0.09375 to 0.09375
- gate_scale: float32 [2, 11520], P(None, 'ra'), may hold values from 0.3 to 3
- value_weight: float32 [2, 4224, 11520], P(None, None, 'ra'), may hold values from -0.09375 to 0.09375
- value_scale: float32 [2, 11520], P(None, 'ra'), may hold values from 0.3 to 3
- gate_taps: float32 [2, 3, 11520], P(None, None, 'ra'), may hold values from -3 to 3
- value_taps: float32 [2, 3, 11520], P(None, None, 'ra'), may hold values from -3 to 3
- down_weight: float32 [2, 11520, 4224], P(None, None, 'ra'), may hold values from -0.0546875 to 0.0546875
- down_scale: float32 [2, 4224], P(None, 'ra'), may hold values from 0.3 to 3
- final_gain: float32 [4224], P('ra'), may hold values from 0.1 to 1.9
Outputs:
- normalized: bfloat16 [512, 4224], P('cb', 'ra')
Inputs may be any that keep to these rules, and one draw needn't show every extreme that they name: `activations`: rows and columns have unequal scales.
All inputs are finite; a program needn't handle non-finite values.
Results may differ from a plain program's by a relative error of at most 0.017.
Values may be sent and summed in bfloat16 or wider, within the bound.
A program may use at most 320 MiB of HBM per device.

v0:
```python
import jax
import jax.numpy as jnp
from jax import lax
from jax.sharding import PartitionSpec as P

D = 4224
epsilon = 1e-06
resid_scale = 0.5


def from_behind(value, axis, by):
    length = lax.axis_size(axis)
    pairs = [(i, i + by) for i in range(length) if 0 <= i + by < length]
    return lax.ppermute(value, axis, pairs)


def conv_local(values_in, earlier, tap_weights):
    seq_len = values_in.shape[0]
    taps = tap_weights.shape[0]
    padded = jnp.concatenate([earlier, values_in], axis=0)
    total = jnp.zeros(values_in.shape, jnp.float32)
    for offset in range(taps):
        total = total + tap_weights[offset] * padded[offset : offset + seq_len]
    return total


def per_device(
    activations,
    norm_gain,
    gate_weight,
    gate_scale,
    value_weight,
    value_scale,
    gate_taps,
    value_taps,
    down_weight,
    down_scale,
    final_gain,
):
    row_count, width_part = activations.shape
    tok_rows = activations
    layer_count = gate_weight.shape[0]
    taps = gate_taps.shape[1]
    for layer_idx in range(layer_count):
        wide_rows = tok_rows.astype(jnp.float32)
        full_rows = lax.all_gather(tok_rows, "ra", axis=1, tiled=True).astype(jnp.float32)
        inv_norm = lax.rsqrt(jnp.mean(full_rows * full_rows, axis=1, keepdims=True) + epsilon)
        scaled = (full_rows * norm_gain[layer_idx]).astype(jnp.bfloat16)
        gate_pre = (
            jnp.dot(
                scaled,
                gate_weight[layer_idx].astype(jnp.bfloat16),
                preferred_element_type=jnp.float32,
            )
            * inv_norm
            * gate_scale[layer_idx]
        )
        value_pre = (
            jnp.dot(
                scaled,
                value_weight[layer_idx].astype(jnp.bfloat16),
                preferred_element_type=jnp.float32,
            )
            * inv_norm
            * value_scale[layer_idx]
        )
        gate_prev, value_prev = from_behind(
            (gate_pre[row_count - taps + 1 :], value_pre[row_count - taps + 1 :]), "cb", 1
        )
        gate_conv = conv_local(gate_pre, gate_prev, gate_taps[layer_idx])
        value_conv = conv_local(value_pre, value_prev, value_taps[layer_idx])
        down_bf = down_weight[layer_idx].astype(jnp.bfloat16)
        hidden = (jax.nn.silu(gate_conv) * value_conv).astype(jnp.bfloat16)
        down = jnp.dot(
            lax.all_gather(hidden, "ra", axis=1, tiled=True),
            down_bf,
            preferred_element_type=jnp.float32,
        )
        tok_rows = (resid_scale * wide_rows + down * down_scale[layer_idx]).astype(jnp.bfloat16)
    wide_rows = tok_rows.astype(jnp.float32)
    sq_final = lax.psum(jnp.sum(wide_rows * wide_rows, axis=1), "ra")
    inv_norm = lax.rsqrt(sq_final[:, None] / D + epsilon)
    return (wide_rows * inv_norm * final_gain).astype(jnp.bfloat16)


def solution(mesh):
    in_specs = (
        P("cb", "ra"),
        P(),
        P(None, None, "ra"),
        P(None, "ra"),
        P(None, None, "ra"),
        P(None, "ra"),
        P(None, None, "ra"),
        P(None, None, "ra"),
        P(None, None, "ra"),
        P(None, "ra"),
        P("ra"),
    )
    out_specs = P("cb", "ra")
    return jax.shard_map(
        per_device, mesh=mesh, in_specs=in_specs, out_specs=out_specs, check_vma=False
    )
```

profile of v0, /device:TPU:0, one launch (start us, length us, event | category | flops | bytes accessed | tf_op | source)
XLA Modules:
  0.0 316.4 jit_solution(9558296523419066182)
XLA Ops:
  6.5 0.0 all-gather.5.cloned.1.call-start
  6.5 0.7 all-gather.5.cloned.1.call-update
  7.3 0.0 all-gather.7.cloned.1.call-start
  7.3 24.9 %convert.12 = bf16[2,4224,1440]{1,2,0:T(8,128)(2,1)} convert(f32[2,4224,1440]{1,2,0:T(8,128)} %param.13) | non-fusion elementwise | flops 12165120 | bytes 72990720 | tf_op jit(solution)/shard_map/convert.5
  32.2 24.9 %convert.13 = bf16[2,4224,1440]{1,2,0:T(8,128)(2,1)} convert(f32[2,4224,1440]{1,2,0:T(8,128)} %param.15) | non-fusion elementwise | flops 12165120 | bytes 72990720 | tf_op jit(solution)/shard_map/convert.4
  57.0 0.0 copy-done.7
  57.1 0.0 copy-done.8
  57.1 0.0 copy-done.6
  57.1 0.1 slice_reduce_fusion
  57.2 0.0 all-gather.5.cloned.1.call-done
  57.3 1.8 fusion.15
  59.1 8.2 %fusion.13 = f32[128,1440]{0,1:T(8,128)S(1)} fusion(bf16[2,4224,1440]{1,2,0:T(8,128)(2,1)} %convert.12, bf16[128,4224]{0,1:T(8,128)(2,1)} %all-gather.5.cloned.1.call-done, f32[4224]{0:T(1024)S(1)} %get-tuple-element.18, f32[1440]{0:T(1024)S(1)} %get-tuple-element.20, f32[128]{0:T(128)S(1)} %add_rsqrt_fusion.2), kind=kOutput, calls=%fused_computation.23 | convolution fusion | flops 1559126016 | bytes 14006912 | tf_op jit(solution)/shard_map/dot_general | solution.py:50
  67.3 0.0 copy-start
  67.3 0.3 slice.188
  67.6 0.3 copy.12
  67.9 2.4 collective-permute-start
  70.2 0.0 copy-done
  70.3 8.0 %fusion.12 = f32[128,1440]{0,1:T(8,128)S(1)} fusion(bf16[2,4224,1440]{1,2,0:T(8,128)(2,1)} %convert.13, bf16[128,4224]{0,1:T(8,128)(2,1)S(1)} %copy-done, f32[4224]{0:T(1024)S(1)} %get-tuple-element.18, f32[1440]{0:T(1024)S(1)} %get-tuple-element.22, f32[128]{0:T(128)S(1)} %add_rsqrt_fusion.2), kind=kOutput, calls=%fused_computation.22 | convolution fusion | flops 1559126016 | bytes 14006912 | tf_op jit(solution)/shard_map/dot_general | solution.py:59
  78.3 0.0 copy-start.4
  78.3 0.0 copy-start.5
  78.3 0.3 slice.192
  78.5 0.3 copy.14
  78.8 4.5 %collective-permute-start.1 = (f32[2,1440]{1,0:T(2,128)S(1)}, f32[2,1440]{1,0:T(2,128)S(1)}, u32[]{:S(2)}, u32[]{:S(2)}) collective-permute-start(f32[2,1440]{1,0:T(2,128)S(1)} %copy.14), channel_id=1, source_target_pairs={{0,1},{1,2},{2,3},{4,5},{5,6},{6,7},{8,9},{9,10},{10,11},{12,13},{... | collective-permute-start | bytes 34568 | tf_op jit(solution)/shard_map/ppermute | solution.py:14
  83.3 0.0 copy-done.4
  83.3 0.0 copy-done.5
  83.3 0.2 slice_reduce_fusion.5
  83.5 0.0 collective-permute-done
  83.5 0.3 copy.13
  83.8 0.3 collective-permute-done.1
  84.1 0.3 copy.15
  84.4 3.3 %fusion.40 = bf16[128,1440]{0,1:T(8,128)(2,1)} fusion(f32[2,1440]{0,1:T(8,128)S(1)} %copy.15, f32[128,1440]{0,1:T(8,128)S(1)} %fusion.12, f32[128,1440]{0,1:T(8,128)S(1)} %fusion.13, f32[2,1440]{0,1:T(8,128)S(1)} %copy.13, f32[1440]{0:T(1024)S(1)} %get-tuple-element.12, f32[1440]{0:T(1024)S(1)} %get-tuple-element.13, f32[1440]{0:T(1024)S(1)} %get-tuple-element.14, ...), kind=kLoop, calls=%fused_computation.58 | loop fusion | flops 3686400 | bytes 1900800 | tf_op jit(solution)/shard_map/convert_element_type | solution.py:73
  87.7 0.0 all-gather.7.cloned.1.call-update
  87.7 0.0 copy-start.9
  87.7 0.0 copy-start.2
  87.7 0.0 all-gather.9.cloned.1.call-start
  87.8 25.0 %convert.14 = bf16[2,11520,528]{1,2,0:T(8,128)(2,1)} convert(f32[2,11520,528]{1,2,0:T(8,128)} %param.19) | non-fusion elementwise | flops 12165120 | bytes 72990720 | tf_op jit(solution)/shard_map/convert.3
  112.8 34.9 %all-gather.7.cloned.1.call-done = bf16[128,11520]{0,1:T(8,128)(2,1)} async-done(((bf16[128,1440]{0,1:T(8,128)(2,1)}), bf16[128,11520]{0,1:T(8,128)(2,1)}) %all-gather.7.cloned.1.call-update) | async-done | bytes 2949136 | tf_op jit(solution)/shard_map/all_gather | solution.py:75
  147.7 9.3 %fusion.24 = bf16[128,528]{0,1:T(8,128)(2,1)} fusion(bf16[128,11520]{0,1:T(8,128)(2,1)} %all-gather.7.cloned.1.call-done, bf16[2,11520,528]{1,2,0:T(8,128)(2,1)} %convert.14, bf16[128,528]{0,1:T(8,128)(2,1)S(1)} %copy-done.2, f32[528]{0:T(1024)S(1)} %get-tuple-element.24), kind=kOutput, calls=%fused_computation.42 | convolution fusion | flops 1557473280 | bytes 15386688 | tf_op jit(solution)/shard_map/dot_general | solution.py:74
  157.0 0.0 all-gather.9.cloned.1.call-update
  157.0 0.2 all-gather.11.cloned.1.call-start
  157.2 39.1 %all-gather.9.cloned.1.call-done = bf16[128,4224]{0,1:T(8,128)(2,1)} async-done(((bf16[128,528]{0,1:T(8,128)(2,1)}), bf16[128,4224]{0,1:T(8,128)(2,1)}) %all-gather.9.cloned.1.call-update) | async-done | bytes 1081360 | tf_op jit(solution)/shard_map/all_gather | solution.py:46
  196.3 1.8 fusion.17
  198.1 8.2 %fusion.11 = f32[128,1440]{0,1:T(8,128)S(1)} fusion(bf16[2,4224,1440]{1,2,0:T(8,128)(2,1)} %convert.12, bf16[128,4224]{0,1:T(8,128)(2,1)} %all-gather.9.cloned.1.call-done, f32[4224]{0:T(1024)S(1)} %get-tuple-element.17, f32[1440]{0:T(1024)S(1)} %get-tuple-element.19, f32[128]{0:T(128)S(1)} %add_rsqrt_fusion.1), kind=kOutput, calls=%fused_computation.21 | convolution fusion | flops 1559126016 | bytes 14006912 | tf_op jit(solution)/shard_map/dot_general | solution.py:50
  206.4 0.3 slice.197
  206.6 0.3 copy.16
  206.9 1.3 collective-permute-start.2
  208.2 0.0 copy-done.1
  208.2 8.0 %fusion.10 = f32[128,1440]{0,1:T(8,128)S(1)} fusion(bf16[2,4224,1440]{1,2,0:T(8,128)(2,1)} %convert.13, bf16[128,4224]{0,1:T(8,128)(2,1)S(1)} %copy-done.1, f32[4224]{0:T(1024)S(1)} %get-tuple-element.17, f32[1440]{0:T(1024)S(1)} %get-tuple-element.21, f32[128]{0:T(128)S(1)} %add_rsqrt_fusion.1), kind=kOutput, calls=%fused_computation.20 | convolution fusion | flops 1559126016 | bytes 14006912 | tf_op jit(solution)/shard_map/dot_general | solution.py:59
  216.2 0.3 slice.201
  216.4 0.3 copy.18
  216.7 4.1 %collective-permute-start.3 = (f32[2,1440]{1,0:T(2,128)S(1)}, f32[2,1440]{1,0:T(2,128)S(1)}, u32[]{:S(2)}, u32[]{:S(2)}) collective-permute-start(f32[2,1440]{1,0:T(2,128)S(1)} %copy.18), channel_id=1, source_target_pairs={{0,1},{1,2},{2,3},{4,5},{5,6},{6,7},{8,9},{9,10},{10,11},{12,13},{... | collective-permute-start | bytes 34568 | tf_op jit(solution)/shard_map/ppermute | solution.py:14
  220.8 0.0 collective-permute-done.2
  220.8 0.3 copy.17
  221.1 0.0 copy-start.3
  221.1 0.5 collective-permute-done.3
  221.6 0.3 copy.19
  221.9 3.3 %fusion.30 = bf16[128,1440]{0,1:T(8,128)(2,1)} fusion(f32[2,1440]{0,1:T(8,128)S(1)} %copy.19, f32[128,1440]{0,1:T(8,128)S(1)} %fusion.10, f32[128,1440]{0,1:T(8,128)S(1)} %fusion.11, f32[2,1440]{0,1:T(8,128)S(1)} %copy.17, f32[1440]{0:T(1024)S(1)} %get-tuple-element.15, f32[1440]{0:T(1024)S(1)} %get-tuple-element.16, f32[1440]{0:T(1024)S(1)} %get-tuple-element.11, ...), kind=kLoop, calls=%fused_computation.48 | loop fusion | flops 3686400 | bytes 1900800 | tf_op jit(solution)/shard_map/convert_element_type | solution.py:73
  225.2 0.0 all-gather.11.cloned.1.call-update
  225.2 57.5 %all-gather.11.cloned.1.call-done = bf16[128,11520]{0,1:T(8,128)(2,1)} async-done(((bf16[128,1440]{0,1:T(8,128)(2,1)}), bf16[128,11520]{0,1:T(8,128)(2,1)}) %all-gather.11.cloned.1.call-update) | async-done | bytes 2949136 | tf_op jit(solution)/shard_map/all_gather | solution.py:75
  282.7 0.0 copy-done.3
  282.7 7.2 %multiply_reduce_fusion = (f32[128]{0:T(128)S(1)}, f32[128,528]{0,1:T(8,128)S(1)}) fusion(f32[528]{0:T(1024)S(1)} %get-tuple-element.23, bf16[128,11520]{0,1:T(8,128)(2,1)} %all-gather.11.cloned.1.call-done, bf16[2,11520,528]{1,2,0:T(8,128)(2,1)} %convert.14, bf16[128,528]{0,1:T(8,128)(2,1)S(1)} %copy-done.3), kind=kOutput, calls=%fused_computation.72 | convolution fusion | flops 1557675904 | bytes 15522368 | tf_op jit(solution)/shard_map/dot_general | solution.py:74
  290.0 19.1 %psum.7 = f32[128]{0:T(128)S(1)} all-reduce(f32[128]{0:T(128)S(1)} %get-tuple-element.25), channel_id=1, replica_groups=mesh['ra'=8,'cb'=4] {'ra'}, use_global_device_ids=true, to_apply=%region_3.4 | all-reduce | flops 128 | bytes 1024 | tf_op jit(solution)/shard_map/psum | solution.py:81
  309.0 0.0 copy-done.10
  309.0 0.8 multiply_convert_fusion
  (13 shorter events, 0.1 us)
Async XLA Ops:
  6.5 50.7 %all-gather.5.cloned.1.call-start = ((), (), s32[]{:S(2)}) async-start(), calls=%async_computation | async-start | bytes 1216512 | tf_op jit(solution)/shard_map/all_gather | solution.py:46
  7.3 140.5 %all-gather.7.cloned.1.call-start = ((), (), s32[]{:S(2)}) async-start(), calls=%async_computation.1 | async-start | bytes 3317760 | tf_op jit(solution)/shard_map/all_gather | solution.py:75
  32.2 24.9 %copy-start.7 = (f32[2,1440]{1,0:T(2,128)S(1)}, f32[2,1440]{1,0:T(2,128)}, u32[]{:S(2)}) copy-start(f32[2,1440]{1,0:T(2,128)} %param.14) | copy-start | bytes 34564
  32.2 24.9 %copy-start.8 = (f32[2,1440]{1,0:T(2,128)S(1)}, f32[2,1440]{1,0:T(2,128)}, u32[]{:S(2)}) copy-start(f32[2,1440]{1,0:T(2,128)} %param.16) | copy-start | bytes 34564
  32.2 25.0 %copy-start.6 = (f32[2,4224]{1,0:T(2,128)S(1)}, f32[2,4224]{1,0:T(2,128)}, u32[]{:S(2)}) copy-start(f32[2,4224]{1,0:T(2,128)} %param.12) | copy-start | bytes 101380
  67.3 2.9 copy-start
  67.9 15.6 %collective-permute-start = (f32[2,1440]{1,0:T(2,128)S(1)}, f32[2,1440]{1,0:T(2,128)S(1)}, u32[]{:S(2)}, u32[]{:S(2)}) collective-permute-start(f32[2,1440]{1,0:T(2,128)S(1)} %copy.12), channel_id=1, source_target_pairs={{0,1},{1,2},{2,3},{4,5},{5,6},{6,7},{8,9},{9,10},{10,11},{12,13},{... | collective-permute-start | bytes 34568 | tf_op jit(solution)/shard_map/ppermute | solution.py:14
  78.3 5.0 %copy-start.4 = (f32[2,3,1440]{2,0,1:T(2,128)S(1)}, f32[2,3,1440]{2,0,1:T(2,128)}, u32[]{:S(2)}) copy-start(f32[2,3,1440]{2,0,1:T(2,128)} %param.18) | copy-start | bytes 103684
  78.3 5.0 %copy-start.5 = (f32[2,3,1440]{2,0,1:T(2,128)S(1)}, f32[2,3,1440]{2,0,1:T(2,128)}, u32[]{:S(2)}) copy-start(f32[2,3,1440]{2,0,1:T(2,128)} %param.17) | copy-start | bytes 103684
  78.8 5.3 %collective-permute-start.1 = (f32[2,1440]{1,0:T(2,128)S(1)}, f32[2,1440]{1,0:T(2,128)S(1)}, u32[]{:S(2)}, u32[]{:S(2)}) collective-permute-start(f32[2,1440]{1,0:T(2,128)S(1)} %copy.14), channel_id=1, source_target_pairs={{0,1},{1,2},{2,3},{4,5},{5,6},{6,7},{8,9},{9,10},{10,11},{12,13},{... | collective-permute-start | bytes 34568 | tf_op jit(solution)/shard_map/ppermute | solution.py:14
  87.7 25.1 %copy-start.9 = (f32[2,528]{1,0:T(2,128)S(1)}, f32[2,528]{1,0:T(2,128)}, u32[]{:S(2)}) copy-start(f32[2,528]{1,0:T(2,128)} %param.20) | copy-start | bytes 12676
  87.7 60.0 %copy-start.2 = (bf16[128,528]{0,1:T(8,128)(2,1)S(1)}, bf16[128,528]{0,1:T(8,128)(2,1)}, u32[]{:S(2)}) copy-start(bf16[128,528]{0,1:T(8,128)(2,1)} %param.11) | copy-start | bytes 405508
  87.7 108.6 %all-gather.9.cloned.1.call-start = ((), (), s32[]{:S(2)}) async-start(), calls=%async_computation.2 | async-start | bytes 1216512 | tf_op jit(solution)/shard_map/all_gather | solution.py:46
  157.0 125.7 %all-gather.11.cloned.1.call-start = ((), (), s32[]{:S(2)}) async-start(), calls=%async_computation.3 | async-start | bytes 3317760 | tf_op jit(solution)/shard_map/all_gather | solution.py:75
  206.4 1.8 copy-start.1
  206.9 13.9 %collective-permute-start.2 = (f32[2,1440]{1,0:T(2,128)S(1)}, f32[2,1440]{1,0:T(2,128)S(1)}, u32[]{:S(2)}, u32[]{:S(2)}) collective-permute-start(f32[2,1440]{1,0:T(2,128)S(1)} %copy.16), channel_id=1, source_target_pairs={{0,1},{1,2},{2,3},{4,5},{5,6},{6,7},{8,9},{9,10},{10,11},{12,13},{... | collective-permute-start | bytes 34568 | tf_op jit(solution)/shard_map/ppermute | solution.py:14
  216.7 4.9 %collective-permute-start.3 = (f32[2,1440]{1,0:T(2,128)S(1)}, f32[2,1440]{1,0:T(2,128)S(1)}, u32[]{:S(2)}, u32[]{:S(2)}) collective-permute-start(f32[2,1440]{1,0:T(2,128)S(1)} %copy.18), channel_id=1, source_target_pairs={{0,1},{1,2},{2,3},{4,5},{5,6},{6,7},{8,9},{9,10},{10,11},{12,13},{... | collective-permute-start | bytes 34568 | tf_op jit(solution)/shard_map/ppermute | solution.py:14
  221.1 61.6 %copy-start.3 = (bf16[128,528]{0,1:T(8,128)(2,1)S(1)}, bf16[128,528]{0,1:T(8,128)(2,1)}, u32[]{:S(2)}) copy-start(bf16[128,528]{0,1:T(8,128)(2,1)} %fusion.24) | copy-start | bytes 405508
  282.7 26.3 %copy-start.10 = (f32[528]{0:T(1024)S(1)}, f32[528]{0:T(1024)}, u32[]{:S(2)}) copy-start(f32[528]{0:T(1024)} %param.21) | copy-start | bytes 6340
Sparse Core Ops, SparseCore 0:
  9.5 43.2 all-gather.4
  87.8 59.8 all-gather.6
  157.1 39.1 all-gather.8
  225.4 57.3 all-gather.10
where the time goes:
time: 317 us; the launch traced here: 316 us
  waiting for transfers between devices  133 us (42%)
  other arithmetic  85.8 us (27%)
  matrix products  48.9 us (15%)
  blocking collectives  19.1 us (6%)
  between operations  13.4 us (4%)
  starting transfers between devices  12.6 us (4%)
  local copies, waits for them, and re-layouts  3.63 us (1%)
    all_gather x2, waiting for transfers between devices, per_device(): lax.all_gather(hidden, 'ra', axis=1, tiled=True)  92.4 us
    another operation x3, other arithmetic  74.7 us
    all_gather x2, waiting for transfers between devices, per_device(): lax.all_gather(tok_rows, 'ra', axis=1, tiled=True).astype(jnp.float32)  39.1 us
    psum x1, blocking collectives, per_device(): sq_final = lax.psum(jnp.sum(wide_rows * wide_rows, axis=1), 'ra')  19.1 us
    dot_general x2, matrix products, per_device(): jnp.dot(scaled, gate_weight[layer_idx].astype(jnp.bfloat16), preferred_el...  16.5 us
    dot_general x2, matrix products, per_device(): jnp.dot(lax.all_gather(hidden, 'ra', axis=1, tiled=True), down_bf, prefer...  16.4 us
    dot_general x2, matrix products, per_device(): jnp.dot(scaled, value_weight[layer_idx].astype(jnp.bfloat16), preferred_e...  16 us
    ppermute x4, starting transfers between devices, from_behind(): return lax.ppermute(value, axis, pairs)  12.2 us
  transfers between devices with their start and end apart: 8, of which 5 were waited for; matrix products, arithmetic and copies ran while one was open for 29% of the time, Pallas kernels for 0%

commit v1 on v0

--- a/solution.py
+++ b/solution.py
@@ -2,6 +2,7 @@
 import jax.numpy as jnp
 from jax import lax
 from jax.sharding import PartitionSpec as P
+from jax.lax import all_gather
 
 D = 4224
 epsilon = 1e-06
@@ -43,7 +44,7 @@
     taps = gate_taps.shape[1]
     for layer_idx in range(layer_count):
         wide_rows = tok_rows.astype(jnp.float32)
-        full_rows = lax.all_gather(tok_rows, "ra", axis=1, tiled=True).astype(jnp.float32)
+        full_rows = jnp.concatenate(all_gather(tok_rows, "ra"), axis=1).astype(jnp.float32)
         inv_norm = lax.rsqrt(jnp.mean(full_rows * full_rows, axis=1, keepdims=True) + epsilon)
         scaled = (full_rows * norm_gain[layer_idx]).astype(jnp.bfloat16)
         gate_pre = (

time: 317 us -> 314 us (level)
  matrix products: 48.9 us -> 41.9 us
    dot_general x2, matrix products: 16.5 us -> 12.7 us  [per_device(): jnp.dot(scaled, gate_weight[layer_idx].astype(jnp.bfloat16), preferred_el...]
    unnamed x0 -> x2, other arithmetic: none -> 3.26 us
    dot_general x2, matrix products: 16 us -> 12.7 us  [per_device(): jnp.dot(scaled, value_weight[layer_idx].astype(jnp.bfloat16), preferred_e...]
where the time goes in v1:
time: 314 us; the launch traced here: 313 us
  waiting for transfers between devices  132 us (42%)
  other arithmetic  87.5 us (28%)
  matrix products  41.9 us (13%)
  blocking collectives  19.1 us (6%)
  between operations  13.4 us (4%)
  starting transfers between devices  12.9 us (4%)
  local copies, waits for them, and re-layouts  5.85 us (2%)
    all_gather x2, waiting for transfers between devices, per_device(): lax.all_gather(hidden, 'ra', axis=1, tiled=True)  92.5 us
    another operation x3, other arithmetic  74.7 us
    all_gather x2, waiting for transfers between devices, per_device(): all_gather(tok_rows, 'ra')  38.3 us
    psum x1, blocking collectives, per_device(): sq_final = lax.psum(jnp.sum(wide_rows * wide_rows, axis=1), 'ra')  19.1 us
    dot_general x2, matrix products, per_device(): jnp.dot(lax.all_gather(hidden, 'ra', axis=1, tiled=True), down_bf, prefer...  16.4 us
    dot_general x2, matrix products, per_device(): jnp.dot(scaled, value_weight[layer_idx].astype(jnp.bfloat16), preferred_e...  12.7 us
    dot_general x2, matrix products, per_device(): jnp.dot(scaled, gate_weight[layer_idx].astype(jnp.bfloat16), preferred_el...  12.7 us
    ppermute x4, starting transfers between devices, from_behind(): return lax.ppermute(value, axis, pairs)  12.7 us
  transfers between devices with their start and end apart: 8, of which 5 were waited for; matrix products, arithmetic and copies ran while one was open for 29% of the time, Pallas kernels for 0%

profile of v1, /device:TPU:0, one launch (start us, length us, event | category | flops | bytes accessed | tf_op | source)
XLA Modules:
  0.0 313.0 jit_solution(1750459362190542594)
XLA Ops:
  6.5 0.7 all-gather.11.cloned.1.call-update
  7.3 0.0 all-gather.7.cloned.1.call-start
  7.3 0.9 slice_reduce_fusion
  8.2 0.1 mul.285
  8.3 0.1 copy.18
  8.5 24.8 %convert.13 = bf16[2,4224,1440]{1,2,0:T(8,128)(2,1)} convert(f32[2,4224,1440]{1,2,0:T(8,128)} %param.15) | non-fusion elementwise | flops 12165120 | bytes 72990720 | tf_op jit(solution)/shard_map/convert.4
  33.3 24.9 %convert.12 = bf16[2,4224,1440]{1,2,0:T(8,128)(2,1)} convert(f32[2,4224,1440]{1,2,0:T(8,128)} %param.13) | non-fusion elementwise | flops 12165120 | bytes 72990720 | tf_op jit(solution)/shard_map/convert.5
  58.2 0.0 copy-done.5
  58.3 0.0 all-gather.11.cloned.1.call-done
  58.3 1.5 convert_bitcast_fusion.2
  59.8 0.5 copy.30
  60.3 0.8 fusion.16
  61.0 0.1 copy.19
  61.2 6.4 %fusion.12 = f32[128,1440]{0,1:T(8,128)S(1)} fusion(bf16[128,4224]{0,1:T(8,128)(2,1)S(1)} %bitcast.89, bf16[2,4224,1440]{1,2,0:T(8,128)(2,1)} %convert.13, f32[1440]{0:T(1024)S(1)} %get-tuple-element.22, f32[128]{0:T(128)S(1)} %add_rsqrt_fusion.2), kind=kOutput, calls=%fused_computation.20 | convolution fusion | flops 1557504000 | bytes 13990016 | tf_op jit(solution)/shard_map/dot_general | solution.py:60
  67.6 0.3 slice.192
  67.8 0.3 copy.22
  68.1 2.4 collective-permute-start.1
  70.5 6.4 %fusion.13 = f32[128,1440]{0,1:T(8,128)S(1)} fusion(bf16[128,4224]{0,1:T(8,128)(2,1)S(1)} %bitcast.90, bf16[2,4224,1440]{1,2,0:T(8,128)(2,1)} %convert.12, f32[1440]{0:T(1024)S(1)} %get-tuple-element.20, f32[128]{0:T(128)S(1)} %add_rsqrt_fusion.2), kind=kOutput, calls=%fused_computation.21 | convolution fusion | flops 1557504000 | bytes 13990016 | tf_op jit(solution)/shard_map/dot_general | solution.py:51
  76.9 0.0 copy-start.2
  76.9 0.0 copy-start.3
  76.9 0.3 slice.188
  77.1 0.3 copy.20
  77.4 4.6 %collective-permute-start = (f32[2,1440]{1,0:T(2,128)S(1)}, f32[2,1440]{1,0:T(2,128)S(1)}, u32[]{:S(2)}, u32[]{:S(2)}) collective-permute-start(f32[2,1440]{1,0:T(2,128)S(1)} %copy.20), channel_id=1, source_target_pairs={{0,1},{1,2},{2,3},{4,5},{5,6},{6,7},{8,9},{9,10},{10,11},{12,13},{... | collective-permute-start | bytes 34568 | tf_op jit(solution)/shard_map/ppermute | solution.py:15
  82.0 0.0 copy-done.2
  82.0 0.2 slice_reduce_fusion.5
  82.2 0.0 collective-permute-done.1
  82.2 0.3 copy.23
  82.5 0.3 collective-permute-done
  82.8 0.3 copy.21
  83.1 3.3 %fusion.40 = bf16[128,1440]{0,1:T(8,128)(2,1)} fusion(f32[2,1440]{0,1:T(8,128)S(1)} %copy.23, f32[128,1440]{0,1:T(8,128)S(1)} %fusion.12, f32[128,1440]{0,1:T(8,128)S(1)} %fusion.13, f32[2,1440]{0,1:T(8,128)S(1)} %copy.21, f32[1440]{0:T(1024)S(1)} %get-tuple-element.12, f32[1440]{0:T(1024)S(1)} %get-tuple-element.13, f32[1440]{0:T(1024)S(1)} %get-tuple-element.14, ...), kind=kLoop, calls=%fused_computation.61 | loop fusion | flops 3686400 | bytes 1900800 | tf_op jit(solution)/shard_map/convert_element_type | solution.py:74
  86.4 0.0 all-gather.7.cloned.1.call-update
  86.4 0.0 copy-start.6
  86.4 0.0 copy-start
  86.4 0.0 all-gather.13.cloned.1.call-start
  86.5 25.0 %convert.14 = bf16[2,11520,528]{1,2,0:T(8,128)(2,1)} convert(f32[2,11520,528]{1,2,0:T(8,128)} %param.19) | non-fusion elementwise | flops 12165120 | bytes 72990720 | tf_op jit(solution)/shard_map/convert.3
  111.5 34.9 %all-gather.7.cloned.1.call-done = bf16[128,11520]{0,1:T(8,128)(2,1)} async-done(((bf16[128,1440]{0,1:T(8,128)(2,1)}), bf16[128,11520]{0,1:T(8,128)(2,1)}) %all-gather.7.cloned.1.call-update) | async-done | bytes 2949136 | tf_op jit(solution)/shard_map/all_gather | solution.py:76
  146.4 9.3 %fusion.24 = bf16[128,528]{0,1:T(8,128)(2,1)} fusion(bf16[128,11520]{0,1:T(8,128)(2,1)} %all-gather.7.cloned.1.call-done, bf16[2,11520,528]{1,2,0:T(8,128)(2,1)} %convert.14, bf16[128,528]{0,1:T(8,128)(2,1)S(1)} %copy-done, f32[528]{0:T(1024)S(1)} %get-tuple-element.24), kind=kOutput, calls=%fused_computation.45 | convolution fusion | flops 1557473280 | bytes 15386688 | tf_op jit(solution)/shard_map/dot_general | solution.py:75
  155.7 0.0 all-gather.13.cloned.1.call-update
  155.7 0.0 all-gather.9.cloned.1.call-start
  155.8 0.1 mul.322
  155.8 38.3 %all-gather.13.cloned.1.call-done = bf16[1024,528]{0,1:T(8,128)(2,1)} async-done(((bf16[128,528]{0,1:T(8,128)(2,1)}), bf16[1024,528]{0,1:T(8,128)(2,1)}) %all-gather.13.cloned.1.call-update) | async-done | bytes 1081360 | tf_op jit(solution)/shard_map/all_gather | solution.py:47
  194.1 1.8 convert_bitcast_fusion.1
  195.9 0.5 copy.31
  196.4 0.6 fusion.14
  197.0 0.8 fusion.17
  197.7 6.4 %fusion.10 = f32[128,1440]{0,1:T(8,128)S(1)} fusion(bf16[128,4224]{0,1:T(8,128)(2,1)S(1)} %bitcast.87, bf16[2,4224,1440]{1,2,0:T(8,128)(2,1)} %convert.13, f32[1440]{0:T(1024)S(1)} %get-tuple-element.21, f32[128]{0:T(128)S(1)} %add_rsqrt_fusion.1), kind=kOutput, calls=%fused_computation.18 | convolution fusion | flops 1557504000 | bytes 13990016 | tf_op jit(solution)/shard_map/dot_general | solution.py:60
  204.1 0.3 slice.201
  204.4 0.3 copy.27
  204.6 1.5 collective-permute-start.3
  206.1 6.4 %fusion.11 = f32[128,1440]{0,1:T(8,128)S(1)} fusion(bf16[128,4224]{0,1:T(8,128)(2,1)S(1)} %bitcast.88, bf16[2,4224,1440]{1,2,0:T(8,128)(2,1)} %convert.12, f32[1440]{0:T(1024)S(1)} %get-tuple-element.19, f32[128]{0:T(128)S(1)} %add_rsqrt_fusion.1), kind=kOutput, calls=%fused_computation.19 | convolution fusion | flops 1557504000 | bytes 13990016 | tf_op jit(solution)/shard_map/dot_general | solution.py:51
  212.5 0.3 slice.197
  212.7 0.3 copy.25
  213.0 4.3 %collective-permute-start.2 = (f32[2,1440]{1,0:T(2,128)S(1)}, f32[2,1440]{1,0:T(2,128)S(1)}, u32[]{:S(2)}, u32[]{:S(2)}) collective-permute-start(f32[2,1440]{1,0:T(2,128)S(1)} %copy.25), channel_id=1, source_target_pairs={{0,1},{1,2},{2,3},{4,5},{5,6},{6,7},{8,9},{9,10},{10,11},{12,13},{... | collective-permute-start | bytes 34568 | tf_op jit(solution)/shard_map/ppermute | solution.py:15
  217.3 0.0 collective-permute-done.3
  217.3 0.3 copy.28
  217.6 0.0 copy-start.1
  217.6 0.5 collective-permute-done.2
  218.1 0.3 copy.26
  218.4 3.3 %fusion.30 = bf16[128,1440]{0,1:T(8,128)(2,1)} fusion(f32[2,1440]{0,1:T(8,128)S(1)} %copy.28, f32[128,1440]{0,1:T(8,128)S(1)} %fusion.10, f32[128,1440]{0,1:T(8,128)S(1)} %fusion.11, f32[2,1440]{0,1:T(8,128)S(1)} %copy.26, f32[1440]{0:T(1024)S(1)} %get-tuple-element.15, f32[1440]{0:T(1024)S(1)} %get-tuple-element.16, f32[1440]{0:T(1024)S(1)} %get-tuple-element.11, ...), kind=kLoop, calls=%fused_computation.51 | loop fusion | flops 3686400 | bytes 1900800 | tf_op jit(solution)/shard_map/convert_element_type | solution.py:74
  221.7 0.0 all-gather.9.cloned.1.call-update
  221.8 57.6 %all-gather.9.cloned.1.call-done = bf16[128,11520]{0,1:T(8,128)(2,1)} async-done(((bf16[128,1440]{0,1:T(8,128)(2,1)}), bf16[128,11520]{0,1:T(8,128)(2,1)}) %all-gather.9.cloned.1.call-update) | async-done | bytes 2949136 | tf_op jit(solution)/shard_map/all_gather | solution.py:76
  279.3 7.2 %multiply_reduce_fusion = (f32[128]{0:T(128)S(1)}, f32[128,528]{0,1:T(8,128)S(1)}) fusion(f32[528]{0:T(1024)S(1)} %get-tuple-element.23, bf16[128,11520]{0,1:T(8,128)(2,1)} %all-gather.9.cloned.1.call-done, bf16[2,11520,528]{1,2,0:T(8,128)(2,1)} %convert.14, bf16[128,528]{0,1:T(8,128)(2,1)S(1)} %copy-done.1), kind=kOutput, calls=%fused_computation.75 | convolution fusion | flops 1557675904 | bytes 15522368 | tf_op jit(solution)/shard_map/dot_general | solution.py:75
  286.5 19.1 %psum.7 = f32[128]{0:T(128)S(1)} all-reduce(f32[128]{0:T(128)S(1)} %get-tuple-element.29), channel_id=1, replica_groups=mesh['ra'=8,'cb'=4] {'ra'}, use_global_device_ids=true, to_apply=%region_3.4 | all-reduce | flops 128 | bytes 1024 | tf_op jit(solution)/shard_map/psum | solution.py:82
  305.6 0.8 multiply_convert_fusion
  (16 shorter events, 0.1 us)
Async XLA Ops:
  6.5 51.7 %all-gather.11.cloned.1.call-start = ((), (), s32[]{:S(2)}) async-start(), calls=%async_computation.2 | async-start | bytes 1216512 | tf_op jit(solution)/shard_map/all_gather | solution.py:47
  7.3 139.2 %all-gather.7.cloned.1.call-start = ((), (), s32[]{:S(2)}) async-start(), calls=%async_computation | async-start | bytes 3317760 | tf_op jit(solution)/shard_map/all_gather | solution.py:76
  33.3 24.9 %copy-start.4 = (f32[2,1440]{1,0:T(2,128)S(1)}, f32[2,1440]{1,0:T(2,128)}, u32[]{:S(2)}) copy-start(f32[2,1440]{1,0:T(2,128)} %param.16) | copy-start | bytes 34564
  33.3 24.9 %copy-start.5 = (f32[2,1440]{1,0:T(2,128)S(1)}, f32[2,1440]{1,0:T(2,128)}, u32[]{:S(2)}) copy-start(f32[2,1440]{1,0:T(2,128)} %param.14) | copy-start | bytes 34564
  68.1 14.1 %collective-permute-start.1 = (f32[2,1440]{1,0:T(2,128)S(1)}, f32[2,1440]{1,0:T(2,128)S(1)}, u32[]{:S(2)}, u32[]{:S(2)}) collective-permute-start(f32[2,1440]{1,0:T(2,128)S(1)} %copy.22), channel_id=1, source_target_pairs={{0,1},{1,2},{2,3},{4,5},{5,6},{6,7},{8,9},{9,10},{10,11},{12,13},{... | collective-permute-start | bytes 34568 | tf_op jit(solution)/shard_map/ppermute | solution.py:15
  76.9 5.1 %copy-start.2 = (f32[2,3,1440]{2,0,1:T(2,128)S(1)}, f32[2,3,1440]{2,0,1:T(2,128)}, u32[]{:S(2)}) copy-start(f32[2,3,1440]{2,0,1:T(2,128)} %param.18) | copy-start | bytes 103684
  76.9 5.1 %copy-start.3 = (f32[2,3,1440]{2,0,1:T(2,128)S(1)}, f32[2,3,1440]{2,0,1:T(2,128)}, u32[]{:S(2)}) copy-start(f32[2,3,1440]{2,0,1:T(2,128)} %param.17) | copy-start | bytes 103684
  77.4 5.4 %collective-permute-start = (f32[2,1440]{1,0:T(2,128)S(1)}, f32[2,1440]{1,0:T(2,128)S(1)}, u32[]{:S(2)}, u32[]{:S(2)}) collective-permute-start(f32[2,1440]{1,0:T(2,128)S(1)} %copy.20), channel_id=1, source_target_pairs={{0,1},{1,2},{2,3},{4,5},{5,6},{6,7},{8,9},{9,10},{10,11},{12,13},{... | collective-permute-start | bytes 34568 | tf_op jit(solution)/shard_map/ppermute | solution.py:15
  86.4 25.1 %copy-start.6 = (f32[2,528]{1,0:T(2,128)S(1)}, f32[2,528]{1,0:T(2,128)}, u32[]{:S(2)}) copy-start(f32[2,528]{1,0:T(2,128)} %param.20) | copy-start | bytes 12676
  86.4 60.0 %copy-start = (bf16[128,528]{0,1:T(8,128)(2,1)S(1)}, bf16[128,528]{0,1:T(8,128)(2,1)}, u32[]{:S(2)}) copy-start(bf16[128,528]{0,1:T(8,128)(2,1)} %param.11) | copy-start | bytes 405508
  86.4 107.7 %all-gather.13.cloned.1.call-start = ((), (), s32[]{:S(2)}) async-start(), calls=%async_computation.3 | async-start | bytes 1216512 | tf_op jit(solution)/shard_map/all_gather | solution.py:47
  155.7 123.6 %all-gather.9.cloned.1.call-start = ((), (), s32[]{:S(2)}) async-start(), calls=%async_computation.1 | async-start | bytes 3317760 | tf_op jit(solution)/shard_map/all_gather | solution.py:76
  204.6 12.7 %collective-permute-start.3 = (f32[2,1440]{1,0:T(2,128)S(1)}, f32[2,1440]{1,0:T(2,128)S(1)}, u32[]{:S(2)}, u32[]{:S(2)}) collective-permute-start(f32[2,1440]{1,0:T(2,128)S(1)} %copy.27), channel_id=1, source_target_pairs={{0,1},{1,2},{2,3},{4,5},{5,6},{6,7},{8,9},{9,10},{10,11},{12,13},{... | collective-permute-start | bytes 34568 | tf_op jit(solution)/shard_map/ppermute | solution.py:15
  213.0 5.1 %collective-permute-start.2 = (f32[2,1440]{1,0:T(2,128)S(1)}, f32[2,1440]{1,0:T(2,128)S(1)}, u32[]{:S(2)}, u32[]{:S(2)}) collective-permute-start(f32[2,1440]{1,0:T(2,128)S(1)} %copy.25), channel_id=1, source_target_pairs={{0,1},{1,2},{2,3},{4,5},{5,6},{6,7},{8,9},{9,10},{10,11},{12,13},{... | collective-permute-start | bytes 34568 | tf_op jit(solution)/shard_map/ppermute | solution.py:15
  217.6 61.7 %copy-start.1 = (bf16[128,528]{0,1:T(8,128)(2,1)S(1)}, bf16[128,528]{0,1:T(8,128)(2,1)}, u32[]{:S(2)}) copy-start(bf16[128,528]{0,1:T(8,128)(2,1)} %fusion.24) | copy-start | bytes 405508
  279.3 26.3 %copy-start.7 = (f32[528]{0:T(1024)S(1)}, f32[528]{0:T(1024)}, u32[]{:S(2)}) copy-start(f32[528]{0:T(1024)} %param.21) | copy-start | bytes 6340
Sparse Core Ops, SparseCore 0:
  9.4 42.3 all-gather.10
  86.5 59.8 all-gather.6
  155.8 38.2 all-gather.12
  221.9 57.4 all-gather.8
